TPU v7x, 32 devices: a whole 2x2x4 slice. The times are simulated.
32 devices in a mesh: sp: 16 (over z, y, x), tp: 2 (over core).
Axes of the slice: x: 2, y: 2, z: 4, core: 2. Of those that a mesh axis runs over, the one named last changes fastest.
Arguments:
- input_activity: bfloat16 [8, 1024, 1024], P(None, ('sp', 'tp')), may hold values from -6 to 6
- norm_gain: bfloat16 [1024], replicated, may hold values from 0.75 to 1.25
- w_query: bfloat16 [1024, 256], P(None, 'tp'), may hold values from -0.1875 to 0.1875
- w_key: bfloat16 [1024, 256], P(None, 'tp'), may hold values from -0.1875 to 0.1875
- w_value: bfloat16 [1024, 512], P(None, 'tp'), may hold values from -0.1875 to 0.1875
- w_gate: bfloat16 [1024, 512], P(None, 'tp'), may hold values from -0.1875 to 0.1875
- head_gain: bfloat16 [4, 128], P('tp'), may hold values from 0.75 to 1.25
- w_out: bfloat16 [512, 1024], P('tp'), may hold values from -0.25 to 0.25
- initial_state: float32 [8, 4, 64, 128], P(None, 'tp'), may hold values from -24 to 24
Outputs:
- output: bfloat16 [8, 1024, 1024], P(None, ('sp', 'tp'))
- closing_memory: float32 [8, 4, 64, 128], P(None, 'tp')
All inputs are finite; a program needn't handle non-finite values.
Results may differ from a plain program's by a relative error of at most 0.015.
Values may be sent and summed in bfloat16 or wider, within the bound.
A program may use at most 64 MiB of HBM per device.

v0:
```python
import jax
import jax.numpy as jnp
from jax import lax
from jax.sharding import PartitionSpec as P

EPS = 1e-06
ROPE_BASE = 10000.0


def gathered_then(slab, axis, dim, apply):
    everything = lax.all_gather(slab, axis, axis=dim, tiled=True)
    return apply(everything, jnp.int32(0))


def carried_in(value, axis, join, neutral, backward):
    count, mine = lax.axis_size(axis), lax.axis_index(axis)
    pieces = jax.tree.map(lambda part: lax.all_gather(part, axis), value)
    if backward:
        pieces = jax.tree.map(lambda part: part[::-1], pieces)
        mine = count - 1 - mine
    so_far = jax.tree.map(
        lambda part, zero: jnp.full_like(part, 0) + jnp.asarray(zero, part.dtype), value, neutral
    )

    def step(position, so_far):
        longer = join(so_far, jax.tree.map(lambda part: part[position], pieces))
        return jax.tree.map(lambda new, old: jnp.where(position < mine, new, old), longer, so_far)

    return lax.fori_loop(0, count - 1, step, so_far)


def summed_rows(product, width, axis):
    everything = product(jnp.int32(0), lax.axis_size(axis) * width)
    own = lax.psum_scatter(everything.astype(jnp.bfloat16), axis, scatter_dimension=0, tiled=True)
    return own.astype(jnp.float32)


def rotate(values_in, places):
    size_last = values_in.shape[-1]
    half = size_last // 2
    freqs = ROPE_BASE ** (-jnp.arange(0, size_last, 2, dtype=jnp.float32) / size_last)
    angle = places[:, None] * freqs[None, :]
    cosine = jnp.cos(angle)[None, :, None, :]
    sine = jnp.sin(angle)[None, :, None, :]
    first = values_in[..., :half]
    second = values_in[..., half:]
    return jnp.concatenate(
        [first * cosine - second * sine, first * sine + second * cosine], axis=-1
    )


def combine(earlier, later):
    return (earlier[0] * later[0], earlier[1] * later[0][None, :, None, None] + later[1])


def on_device(
    input_activity, norm_gain, w_query, w_key, w_value, w_gate, head_gain, w_out, initial_state
):
    seq_count, half_rows, model_width = input_activity.shape
    stretch = half_rows * lax.axis_size("tp")
    local_heads = initial_state.shape[1]
    key_dim = initial_state.shape[2]
    value_dim = initial_state.shape[3]
    floats = input_activity.astype(jnp.float32)
    scaled_unit = (
        floats
        * lax.rsqrt(jnp.mean(floats * floats, axis=-1, keepdims=True) + EPS)
        * norm_gain.astype(jnp.float32)
    ).astype(jnp.bfloat16)
    glued_together = jnp.concatenate([w_query, w_key, w_value, w_gate], axis=1)

    def project(segment_slice, start):
        return jnp.einsum(
            "nqe,ef->nqf", segment_slice, glued_together, preferred_element_type=jnp.float32
        ).astype(jnp.bfloat16)

    projected = gathered_then(scaled_unit, "tp", 1, project)
    key_cols = local_heads * key_dim
    value_cols = local_heads * value_dim
    queries = projected[..., :key_cols].reshape(seq_count, stretch, local_heads, key_dim)
    keys_all = projected[..., key_cols : 2 * key_cols].reshape(
        seq_count, stretch, local_heads, key_dim
    )
    values_all = projected[..., 2 * key_cols : 2 * key_cols + value_cols].reshape(
        seq_count, stretch, local_heads, value_dim
    )
    gates = projected[..., 2 * key_cols + value_cols :].reshape(
        seq_count, stretch, local_heads, value_dim
    )
    places = (lax.axis_index("sp") * stretch + jnp.arange(stretch)).astype(jnp.float32)
    rot_query = rotate(queries.astype(jnp.float32), places).astype(jnp.bfloat16)
    rot_key = (rotate(keys_all.astype(jnp.float32), places) * key_dim ** (-0.5)).astype(
        jnp.bfloat16
    )
    head_ids = (lax.axis_index("tp") * local_heads + jnp.arange(local_heads)).astype(jnp.float32)
    total_len = stretch * lax.axis_size("sp")
    log_decay = -(0.25 + 0.25 * head_ids) / total_len
    steps_idx = jnp.arange(stretch, dtype=jnp.float32)
    start_positions = steps_idx[:, None] - steps_idx[None, :]
    mask = jnp.where(
        start_positions[None] >= 0,
        jnp.exp(jnp.maximum(start_positions, 0.0)[None] * log_decay[:, None, None]),
        0.0,
    )
    key_decay = jnp.exp((stretch - 1 - steps_idx)[None, :] * log_decay[:, None])
    query_decay = jnp.exp((steps_idx + 1.0)[None, :] * log_decay[:, None])
    block_decay = jnp.exp(stretch * log_decay)
    weighted_key = (rot_key.astype(jnp.float32) * key_decay.T[None, :, :, None]).astype(
        jnp.bfloat16
    )
    local_state = jnp.einsum(
        "schd,sche->shde", weighted_key, values_all, preferred_element_type=jnp.float32
    )
    identity = (jnp.ones_like(block_decay), jnp.zeros_like(local_state))
    prefix_decay, earlier_memory = carried_in(
        (block_decay, local_state), "sp", combine, identity, False
    )
    incoming = earlier_memory + prefix_decay[None, :, None, None] * initial_state
    scores = (
        jnp.einsum("schd,skhd->shck", rot_query, rot_key, preferred_element_type=jnp.float32)
        * mask[None]
    )
    inner = jnp.einsum(
        "shck,skhe->sche",
        scores.astype(jnp.bfloat16),
        values_all,
        preferred_element_type=jnp.float32,
    )
    scaled_query = rot_query.astype(jnp.float32) * query_decay.T[None, :, :, None]
    cross = jnp.einsum("schd,shde->sche", scaled_query, incoming, precision=lax.Precision.HIGHEST)
    retained = inner + cross
    centre = jnp.mean(retained, axis=-1, keepdims=True)
    spread = jnp.mean(jnp.square(retained - centre), axis=-1, keepdims=True)
    normalized = (
        (retained - centre) * lax.rsqrt(spread + EPS) * head_gain.astype(jnp.float32)[None, None]
    )
    mixed = (
        (jax.nn.silu(gates.astype(jnp.float32)) * normalized)
        .astype(jnp.bfloat16)
        .reshape(seq_count, stretch, value_cols)
    )
    token_major = mixed.transpose(1, 0, 2)

    def output_rows(start, count):
        rows_here = lax.dynamic_slice_in_dim(token_major, start, count, 0)
        return jnp.einsum("bsm,md->bsd", rows_here, w_out, preferred_element_type=jnp.float32)

    summed = summed_rows(output_rows, half_rows, "tp")
    output = summed.astype(jnp.bfloat16).transpose(1, 0, 2)
    remaining = (lax.axis_size("sp") - 1 - lax.axis_index("sp")).astype(jnp.float32)
    factor = jnp.exp(log_decay * stretch * remaining)
    total = lax.psum(local_state * factor[None, :, None, None], "sp")
    closing_memory = total + initial_state * jnp.exp(log_decay * total_len)[None, :, None, None]
    return (output, closing_memory)


def solution(mesh):
    placed = (
        P(None, ("sp", "tp"), None),
        P(),
        P(None, "tp"),
        P(None, "tp"),
        P(None, "tp"),
        P(None, "tp"),
        P("tp", None),
        P("tp", None),
        P(None, "tp", None, None),
    )
    return jax.shard_map(
        on_device,
        mesh=mesh,
        in_specs=placed,
        out_specs=(P(None, ("sp", "tp"), None), P(None, "tp", None, None)),
        check_vma=False,
    )
```

profile of v0, /device:TPU:0, one launch (start us, length us, event | category | flops | bytes accessed | tf_op | source)
XLA Modules:
  0.0 274.7 jit_solution(17826887981686858333)
XLA Ops:
  7.2 1.3 fusion.12
  9.2 2.0 fusion.14
  11.7 11.5 %all-gather.5.cloned.1.call-done = bf16[8,64,1024]{2,1,0:T(8,128)(2,1)} async-done(((bf16[8,32,1024]{2,1,0:T(8,128)(2,1)}), bf16[8,64,1024]{2,1,0:T(8,128)(2,1)}) %all-gather.5.cloned.1.call-update) | async-done | bytes 1048592 | tf_op jit(solution)/shard_map/all_gather | solution.py:11
  23.2 2.6 fusion.8
  28.3 1.3 broadcast_multiply_fusion
  29.8 41.1 %all-gather.1 = f32[16,1,2]{2,1,0:T(1,128)S(1)} all-gather(f32[1,1,2]{2,1,0:T(1,128)S(1)} %exponential_bitcast_fusion), channel_id=1, replica_groups=mesh['sp'=16,'tp'=2] {'sp'}, dimensions={0}, use_global_device_ids=true | all-gather | bytes 136 | tf_op jit(solution)/shard_map/all_gather | solution.py:17
  71.5 71.7 %all-gather.7.cloned.1.call-done = f32[128,2,64,128]{3,2,1,0:T(8,128)} async-done(((f32[8,2,64,128]{3,2,1,0:T(8,128)}), f32[128,2,64,128]{3,2,1,0:T(8,128)}) %all-gather.7.cloned.1.call-update) | async-done | bytes 8388624 | tf_op jit(solution)/shard_map/all_gather | solution.py:17
  143.2 18.6 %while.16 = (s32[]{:T(128)}, f32[2]{0:T(128)S(1)}, f32[8,2,64,128]{3,2,1,0:T(8,128)S(1)}, s32[]{:T(128)}, f32[16,2]{1,0:T(8,128)S(1)}, /*index=5*/f32[16,8,2,64,128]{4,3,2,1,0:T(8,128)}, s32[]{:T(128)}, s32[]{:T(128)}) while((s32[]{:T(128)}, f32[2]{0:T(128)S(1)}, f32[8,2,64,128]{3,2,1,0:T(8,128)S(1)}, s32[]{:T(128)}, ...), condition=%wide.region_2.3_spmd.clone, body=%wide.region_1.2_spmd.clone.sunk | while | flops 524298 | bytes 1573019 | solution.py:29
  143.3 1.2 fusion.51
  144.5 1.2 fusion.51
  145.8 1.2 fusion.51
  147.0 1.2 fusion.51
  148.3 1.2 fusion.51
  149.5 1.2 fusion.51
  150.7 1.2 fusion.51
  154.4 1.2 fusion.51
  155.7 1.2 fusion.51
  156.9 1.2 fusion.51
  158.1 1.2 fusion.51
  163.6 1.4 convolution_convert_fusion
  165.1 91.3 %all-reduce.2.cloned.1.call-done = f32[8,2,64,128]{3,2,1,0:T(8,128)} async-done(((f32[8,2,64,128]{3,2,1,0:T(8,128)}), f32[8,2,64,128]{3,2,1,0:T(8,128)}) %all-reduce.2.cloned.1.call-update) | async-done | bytes 524304 | tf_op jit(solution)/shard_map/psum | solution.py:152
  256.4 2.0 multiply_add_fusion
  258.4 7.7 %reduce-scatter.2.cloned.1.call-done = bf16[32,8,1024]{2,1,0:T(8,128)(2,1)} async-done(((bf16[64,8,1024]{2,1,0:T(8,128)(2,1)}), bf16[32,8,1024]{2,1,0:T(8,128)(2,1)}) %reduce-scatter.2.cloned.1.call-update) | async-done | bytes 524304 | tf_op jit(solution)/shard_map/reduce_scatter | solution.py:34
  266.1 2.1 copy.50
  (63 shorter events, 11.0 us)
Async XLA Ops:
  7.2 156.4 %copy-start = (bf16[256,1024]{1,0:T(8,128)(2,1)S(1)}, bf16[256,1024]{1,0:T(8,128)(2,1)}, u32[]{:S(2)}) copy-start(bf16[256,1024]{1,0:T(8,128)(2,1)} %param.18) | copy-start | bytes 1572868
  7.2 16.0 %all-gather.5.cloned.1.call-start = ((), (), s32[]{:S(2)}) async-start(), calls=%async_computation.1 | async-start | bytes 1572864 | tf_op jit(solution)/shard_map/all_gather | solution.py:11
  11.2 132.0 %all-gather.7.cloned.1.call-start = ((), (), s32[]{:S(2)}) async-start(), calls=%async_computation.4 | async-start | bytes 8912896 | tf_op jit(solution)/shard_map/all_gather | solution.py:17
  27.8 2.0 copy-start.2
  29.7 226.7 %all-reduce.2.cloned.1.call-start = ((), (), s32[]{:S(2)}) async-start(), calls=%async_computation.3 | async-start | bytes 1048576 | tf_op jit(solution)/shard_map/psum | solution.py:152
  71.0 195.1 %reduce-scatter.2.cloned.1.call-start = ((), (), s32[]{:S(2)}) async-start(), calls=%async_computation.2 | async-start | bytes 1572864 | tf_op jit(solution)/shard_map/reduce_scatter | solution.py:34
  143.2 18.6 %copy-start.1 = (f32[8,2,64,128]{3,2,1,0:T(8,128)S(1)}, f32[8,2,64,128]{3,2,1,0:T(8,128)}, u32[]{:S(2)}) copy-start(f32[8,2,64,128]{3,2,1,0:T(8,128)} %param.19) | copy-start | bytes 1572868
Sparse Core Ops, SparseCore 0:
  11.4 11.7 all-gather.4
  29.8 113.3 all-gather.6
  148.9 107.4 all-reduce.1
  258.5 7.5 reduce-scatter.1
where the time goes:
time: 276 us; the launch traced here: 275 us
  waiting for transfers between devices  182 us (66%)
  blocking collectives  41.1 us (15%)
  other arithmetic  25.9 us (9%)
  between operations  14 us (5%)
  matrix products  6.79 us (2%)
  local copies, waits for them, and re-layouts  3.96 us (1%)
    psum x1, waiting for transfers between devices, on_device(): total = lax.psum(local_state * factor[None, :, None, None], 'sp')  91.3 us
    all_gather x1, waiting for transfers between devices, carried_in(): pieces = jax.tree.map(lambda part: lax.all_gather(part, axis), value)  71.7 us
    all_gather x1, blocking collectives, carried_in(): pieces = jax.tree.map(lambda part: lax.all_gather(part, axis), value)  41.1 us
    select_n x30, other arithmetic, step(): jnp.where(position < mine, new, old)  18.1 us
    all_gather x1, waiting for transfers between devices, gathered_then(): everything = lax.all_gather(slab, axis, axis=dim, tiled=True)  11.5 us
    reduce_scatter x1, waiting for transfers between devices, summed_rows(): lax.psum_scatter(everything.astype(jnp.bfloat16), axis, scatter_dimension...  7.7 us
  transfers between devices with their start and end apart: 4, of which 4 were waited for; matrix products, arithmetic and copies ran while one was open for 9% of the time, Pallas kernels for 0%

commit v1 on v0

v1 whole, which is shorter than its diff:
```python
import functools
import math

import jax
import jax.numpy as jnp
from jax import lax
from jax.experimental import pallas as pl
from jax.experimental.pallas import tpu as pltpu
from jax.sharding import PartitionSpec as P

EPS = 1e-06
ROPE_BASE = 10000.0
MESH = pl.DeviceIdType.MESH
F32, BF16 = jnp.float32, jnp.bfloat16


def kernel(dims, *refs):
    (n_sp, n_tp, plane, column, heads) = dims
    (x_hbm, gain_hbm, wq_hbm, wk_hbm, wv_hbm, wg_hbm, hgain_hbm, wo_hbm, init_hbm) = refs[:9]
    out_ref, closing_ref = refs[9:11]
    (xbuf, gain, wbuf, hgain, wobuf, initb, nbuf, qm, km, kw, vs, gs, inner, lb, ra, sb, rb, sc, rc, sd, rd,
     mx, mr, lsem, xs, xr, ws, wr, as_, ar, bs, br, cs, cr, ds_, dr, ms, mrs) = refs[11:]
    seqs, half, width = x_hbm.shape
    stretch = half * n_tp
    dk = wq_hbm.shape[1] // heads
    dv = wv_hbm.shape[1] // heads
    kc, vc = heads * dk, heads * dv
    group = (seqs * heads) // plane
    total_len = stretch * n_sp
    rows_half = heads * half
    rows = n_tp * rows_half

    me, t_me = lax.axis_index("sp"), lax.axis_index("tp")
    z_me, p_me = me // plane, me % plane

    barrier = pltpu.get_barrier_semaphore()

    def in_plane(o):
        j = (p_me + o) % plane
        return j, (z_me * plane + j, t_me)

    def in_column(o):
        j = (z_me + o) % column
        return j, (j * plane + p_me, t_me)

    def in_chip(o):
        j = (t_me + o) % n_tp
        return j, (me, j)

    peers = [in_chip(o) for o in range(1, n_tp)]
    peers += [in_plane(o) for o in range(1, plane)]
    peers += [in_column(o) for o in range(1, column)]
    for _, where in peers:
        pl.semaphore_signal(barrier, inc=1, device_id=where, device_id_type=MESH)

    def remote(src, dst, s, r, where):
        return pltpu.make_async_remote_copy(
            src_ref=src, dst_ref=dst, send_sem=s, recv_sem=r, device_id=where, device_id_type=MESH
        )

    loads = [
        (x_hbm, xbuf.at[t_me]),
        (gain_hbm, gain),
        (wq_hbm, wbuf.at[:, 0:kc]),
        (wk_hbm, wbuf.at[:, kc : 2 * kc]),
        (wv_hbm, wbuf.at[:, 2 * kc : 2 * kc + vc]),
        (wg_hbm, wbuf.at[:, 2 * kc + vc :]),
        (hgain_hbm, hgain),
        (init_hbm.at[p_me], initb),
        (wo_hbm, wobuf.at[t_me]),
    ]
    local = [pltpu.make_async_copy(a, b, lsem.at[i]) for i, (a, b) in enumerate(loads)]
    for c in local:
        c.start()

    def fiota(shape, dim):
        return lax.broadcasted_iota(jnp.int32, shape, dim).astype(F32)

    def lg_of(head):
        return (-0.25 / total_len) * (1.0 + (t_me * heads).astype(F32) + head)

    lane = fiota((half, kc), 1)
    lane_head = jnp.floor((lane + 0.5) * (1.0 / dk))
    in_head = lane - dk * lane_head
    upper = jnp.floor((in_head + 0.5) * (2.0 / dk))
    freq = jnp.exp((in_head - upper * (dk // 2)) * (-2.0 * math.log(ROPE_BASE) / dk))
    sign = 2.0 * upper - 1.0
    lane_lg = lg_of(lane_head)
    sub = fiota((half, kc), 0)

    ri, ci = fiota((rows, rows), 0), fiota((rows, rows), 1)

    def places_of(i):
        t = jnp.floor((i + 0.5) * (1.0 / rows_half))
        rest = i - t * rows_half
        h = jnp.floor((rest + 0.5) * (1.0 / half))
        return t * half + rest - h * half, h

    (rpos, rhead), (cpos, chead) = places_of(ri), places_of(ci)
    gap = rpos - cpos
    mask = jnp.where(
        jnp.logical_and(rhead == chead, gap >= 0.0),
        jnp.exp(jnp.maximum(gap, 0.0) * lg_of(rhead)),
        0.0,
    )
    inner_decay = mask

    pl.semaphore_wait(barrier, len(peers))

    sends = []
    for o in range(1, n_tp):
        j, where = in_chip(o)
        sends.append(remote(x_hbm, xbuf.at[t_me], xs.at[j], xr.at[t_me], where))
        sends.append(remote(wo_hbm, wobuf.at[t_me], ws.at[j], wr.at[t_me], where))
    for c in sends:
        c.start()

    for c in local[:6]:
        c.wait()

    def project(t):
        for s in range(seqs):
            xf = xbuf[t, s].astype(F32)
            ms_ = jnp.mean(xf * xf, axis=-1, keepdims=True)
            nbuf[s * half : (s + 1) * half, :] = (
                xf * lax.rsqrt(ms_ + EPS) * gain[...].astype(F32)
            ).astype(BF16)
        pos0 = (t * half).astype(F32)
        angle = (me * stretch).astype(F32) + pos0 + sub
        angle = angle * freq
        cosine, sine = jnp.cos(angle)[None], (jnp.sin(angle) * sign)[None]
        keyd = jnp.exp((stretch - 1.0 - pos0 - sub) * lane_lg)[None]

        def piece(lo, hi):
            y = jnp.dot(nbuf[...], wbuf[:, lo:hi], preferred_element_type=F32)
            return y.astype(BF16)

        qk = piece(0, 2 * kc).astype(F32)

        def turn(v):
            v = v.reshape(seqs, half, kc)
            down = pltpu.roll(v, dk // 2, 2)
            up = pltpu.roll(v, kc - dk // 2, 2)
            return v * cosine + jnp.where(upper[None] > 0.5, down, up) * sine

        rq = turn(qk[:, :kc]).astype(BF16).astype(F32)
        rk = (turn(qk[:, kc:]) * dk**-0.5).astype(BF16).astype(F32)
        wkey = rk * keyd
        v = piece(2 * kc, 2 * kc + vc)
        g = piece(2 * kc + vc, 2 * kc + 2 * vc)
        for h in range(heads):
            keep = jnp.where(lane_head == float(h), 1.0, 0.0)[None]
            at = pl.ds(pl.multiple_of(t * rows_half + h * half, half), half)
            qm[:, at, :] = (rq * keep).astype(BF16)
            km[:, at, :] = (rk * keep).astype(BF16)
            kw[:, at, :] = (wkey * keep).astype(BF16)
            vs[:, at, :] = v[:, h * dv : (h + 1) * dv].reshape(seqs, half, dv)
            gs[:, at, :] = g[:, h * dv : (h + 1) * dv].reshape(seqs, half, dv)

    project(t_me)
    for o in range(1, n_tp):
        j, where = in_chip(o)
        remote(x_hbm, xbuf.at[j], xs.at[j], xr.at[j], where).wait_recv()
        project(j)

    for s in range(seqs):
        state = lax.dot_general(
            kw[s], vs[s], (((0,), (0,)), ((), ())), preferred_element_type=F32
        ).astype(BF16)
        for h in range(heads):
            c = s * heads + h
            lb[c // group, c % group] = state[h * dk : (h + 1) * dk]

    for o in range(1, plane):
        j, where = in_plane(o)
        c = remote(lb.at[j], ra.at[p_me], as_.at[j], ar.at[p_me], where)
        c.start()
        sends.append(c)

    for s in range(seqs):
        scores = lax.dot_general(
            qm[s], km[s], (((1,), (1,)), ((), ())), preferred_element_type=F32
        )
        scores = (scores * inner_decay).astype(BF16)
        inner[s] = jnp.dot(scores, vs[s], preferred_element_type=F32)

    ra[p_me] = lb[p_me]
    for c in local[6:]:
        c.wait()

    group_lg = []
    for g in range(group):
        head = ((p_me * group + g) % heads).astype(F32)
        group_lg.append(lg_of(head) * stretch)

    def power(g, k):
        return jnp.exp(jnp.broadcast_to(group_lg[g] * k, (1, dv)))

    one_block = [power(g, 1.0) for g in range(group)]

    for o in range(1, plane):
        j, where = in_plane(o)
        remote(lb.at[j], ra.at[j], as_.at[j], ar.at[j], where).wait_recv()
    for g in range(group):
        acc = ra[0, g].astype(F32)
        for p in range(1, plane):
            acc = acc * one_block[g] + ra[p, g].astype(F32)
        sb[g] = acc.astype(BF16)
    for o in range(1, column):
        j, where = in_column(o)
        c = remote(sb, rb.at[z_me], bs.at[j], br.at[z_me], where)
        c.start()
        sends.append(c)
    rb[z_me] = sb[...]

    zf = z_me.astype(F32)
    before = [
        [
            power(g, plane * jnp.maximum(zf - 1.0 - z, 0.0)) * jnp.where(z < z_me, 1.0, 0.0)
            for z in range(column)
        ]
        for g in range(group)
    ]
    first = [power(g, plane * zf) for g in range(group)]
    after = [[power(g, float(plane * (column - 1 - z))) for z in range(column)] for g in range(group)]
    whole = [power(g, float(plane * column)) for g in range(group)]

    for o in range(1, column):
        j, where = in_column(o)
        remote(sb, rb.at[j], bs.at[j], br.at[j], where).wait_recv()
    for g in range(group):
        start = initb[g]
        incoming = start * first[g]
        total = start * whole[g]
        for z in range(column):
            a = rb[z, g].astype(F32)
            incoming = incoming + a * before[g][z]
            total = total + a * after[g][z]
        for p in range(plane):
            sc[p, g] = incoming.astype(BF16)
            if p < plane - 1:
                incoming = incoming * one_block[g] + ra[p, g].astype(F32)
        sd[g] = total.astype(BF16)
    for o in range(1, plane):
        j, where = in_plane(o)
        c = remote(sc.at[j], rc.at[p_me], cs.at[j], cr.at[p_me], where)
        c.start()
        sends.append(c)
    for o in range(1, plane):
        j, where = in_plane(o)
        c = remote(sd, rd.at[p_me], ds_.at[j], dr.at[p_me], where)
        c.start()
        sends.append(c)
    rc[p_me] = sc[p_me]
    rd[p_me] = sd[...]

    gain_rows = jnp.concatenate(
        [
            jnp.broadcast_to(hgain[h : h + 1, :].astype(F32), (half, dv))
            for h in range(heads)
        ],
        axis=0,
    )

    for o in range(1, plane):
        j, where = in_plane(o)
        remote(sc.at[j], rc.at[j], cs.at[j], cr.at[j], where).wait_recv()

    def finish(t):
        at = pl.ds(pl.multiple_of(t * rows_half, rows_half), rows_half)
        hpos, hhead = places_of(fiota((rows_half, dv), 0))
        decay = jnp.exp((hpos + (t * half).astype(F32) + 1.0) * lg_of(hhead))
        for s in range(seqs):
            memory = jnp.concatenate(
                [rc[(s * heads + h) // group, (s * heads + h) % group] for h in range(heads)], axis=0
            )
            cross = jnp.dot(qm[s, at, :], memory, preferred_element_type=F32)
            kept = inner[s, at, :] + cross * decay
            centre = jnp.mean(kept, axis=-1, keepdims=True)
            kept = kept - centre
            spread = jnp.mean(kept * kept, axis=-1, keepdims=True)
            gate = gs[s, at, :].astype(F32)
            gate = gate * jax.nn.sigmoid(gate)
            mx[t, s] = (gate * (kept * lax.rsqrt(spread + EPS) * gain_rows)).astype(BF16)

    for o in range(1, n_tp):
        j, where = in_chip(o)
        finish(j)
        c = remote(mx.at[j], mr.at[t_me], ms.at[j], mrs.at[t_me], where)
        c.start()
        sends.append(c)
    finish(t_me)
    mr[t_me] = mx[t_me]

    for o in range(1, plane):
        j, where = in_plane(o)
        remote(sd, rd.at[j], ds_.at[j], dr.at[j], where).wait_recv()
    closing_ref[...] = rd[...].astype(F32)

    for o in range(1, n_tp):
        j, where = in_chip(o)
        remote(wo_hbm, wobuf.at[j], ws.at[j], wr.at[j], where).wait_recv()
        remote(mx.at[j], mr.at[j], ms.at[j], mrs.at[j], where).wait_recv()
    side = jnp.concatenate(
        [
            mr[t, :, h * half : (h + 1) * half, :].reshape(seqs * half, dv)
            for t in range(n_tp)
            for h in range(heads)
        ],
        axis=1,
    )
    weight = wobuf[...].reshape(n_tp * vc, width)
    out_ref[...] = (
        jnp.dot(side, weight, preferred_element_type=F32).astype(BF16).reshape(seqs, half, width)
    )
    for c in sends:
        c.wait_send()


def on_device(n_sp, n_tp, x, gain, wq, wk, wv, wg, hgain, wo, init):
    seqs, half, width = x.shape
    heads, dk, dv = init.shape[1:]
    column = 4 if n_sp % 4 == 0 else 1
    plane = n_sp // column
    group = seqs * heads // plane
    rows = n_tp * heads * half
    kc, vc = heads * dk, heads * dv
    any_spec = pl.BlockSpec(memory_space=pl.ANY)
    vmem_spec = pl.BlockSpec(memory_space=pltpu.VMEM)
    V, D = pltpu.VMEM, pltpu.SemaphoreType.DMA
    state = (group, dk, dv)
    out, closing = pl.pallas_call(
        functools.partial(kernel, (n_sp, n_tp, plane, column, heads)),
        out_shape=(
            jax.ShapeDtypeStruct((seqs, half, width), BF16),
            jax.ShapeDtypeStruct((plane,) + state, F32),
        ),
        in_specs=[any_spec] * 9,
        out_specs=(vmem_spec, vmem_spec),
        scratch_shapes=[
            V((n_tp, seqs, half, width), BF16),
            V((1, width), BF16),
            V((width, 2 * kc + 2 * vc), BF16),
            V((heads, dv), BF16),
            V((n_tp, vc, width), BF16),
            V(state, F32),
            V((seqs * half, width), BF16),
            V((seqs, rows, kc), BF16),
            V((seqs, rows, kc), BF16),
            V((seqs, rows, kc), BF16),
            V((seqs, rows, dv), BF16),
            V((seqs, rows, dv), BF16),
            V((seqs, rows, dv), F32),
            V((plane,) + state, BF16),
            V((plane,) + state, BF16),
            V(state, BF16),
            V((column,) + state, BF16),
            V((plane,) + state, BF16),
            V((plane,) + state, BF16),
            V(state, BF16),
            V((plane,) + state, BF16),
            V((n_tp, seqs, heads * half, dv), BF16),
            V((n_tp, seqs, heads * half, dv), BF16),
            D((9,)),
            D((n_tp,)), D((n_tp,)), D((n_tp,)), D((n_tp,)),
            D((plane,)), D((plane,)),
            D((column,)), D((column,)),
            D((plane,)), D((plane,)),
            D((plane,)), D((plane,)),
            D((n_tp,)), D((n_tp,)),
        ],
        compiler_params=pltpu.CompilerParams(collective_id=0, has_side_effects=True),
    )(x, gain.reshape(1, width), wq, wk, wv, wg, hgain, wo, init.reshape((plane,) + state))
    return out, closing.reshape(init.shape)


def solution(mesh):
    placed = (
        P(None, ("sp", "tp"), None),
        P(),
        P(None, "tp"),
        P(None, "tp"),
        P(None, "tp"),
        P(None, "tp"),
        P("tp", None),
        P("tp", None),
        P(None, "tp", None, None),
    )
    return jax.shard_map(
        functools.partial(on_device, mesh.shape["sp"], mesh.shape["tp"]),
        mesh=mesh,
        in_specs=placed,
        out_specs=(P(None, ("sp", "tp"), None), P(None, "tp", None, None)),
        check_vma=False,
    )
```

time: 276 us -> 33 us (0.12)
  waiting for transfers between devices: 182 us -> 0 us
  blocking collectives: 41.1 us -> 0 us
  Pallas kernels: 0 us -> 28.1 us
  other arithmetic: 25.9 us -> 0 us
  between operations: 14 us -> 0.65 us
  matrix products: 6.79 us -> 0 us
    psum x1 -> x0, waiting for transfers between devices: 91.3 us -> none  [on_device(): total = lax.psum(local_state * factor[None, :, None, None], 'sp')]
    all_gather x2 -> x0, waiting for transfers between devices: 83.3 us -> none  [the longest x1 71.7 us: carried_in(): pieces = jax.tree.map(lambda part: lax.all_gather(part, axis), value)]
    all_gather x1 -> x0, blocking collectives: 41.1 us -> none  [carried_in(): pieces = jax.tree.map(lambda part: lax.all_gather(part, axis), value)]
    pallas_call x0 -> x1, Pallas kernels: none -> 28.1 us  [on_device(): pl.pallas_call(functools.partial(kernel, (n_sp, n_tp, plane, column, head...]
    select_n x31 -> x0, other arithmetic: 18.2 us -> none  [the longest x30 18.1 us: step(): jnp.where(position < mine, new, old)]
    reduce_scatter x1 -> x0, waiting for transfers between devices: 7.7 us -> none  [summed_rows(): lax.psum_scatter(everything.astype(jnp.bfloat16), axis, scatter_dimension...]
    dot_general x5 -> x0, matrix products: 6.79 us -> none  [the longest x1 2.63 us: project(): jnp.einsum('nqe,ef->nqf', segment_slice, glued_together, preferred_elemen...]
    convert_element_type x6 -> x0, other arithmetic: 2.96 us -> none  [the longest x1 2.02 us: on_device(): scaled_unit = (floats * lax.rsqrt(jnp.mean(floats * floats, axis=-1, keep...]
  transfers between devices with their start and end apart: 4 -> 0, of which waited for: 4 -> 0; matrix products, arithmetic and copies ran while one was open for 9% -> 0% of each run, Pallas kernels for 0% -> 0%
where the time goes in v1:
time: 33 us; the launch traced here: 32.8 us
  Pallas kernels  28.1 us (85%)
  local copies, waits for them, and re-layouts  4 us (12%)
  between operations  0.65 us (2%)
    pallas_call x1, Pallas kernels, on_device(): pl.pallas_call(functools.partial(kernel, (n_sp, n_tp, plane, column, head...  28.1 us
    unnamed x4, local copies, waits for them, and re-layouts  2.72 us
    reshape x1, local copies, waits for them, and re-layouts, on_device(): gain.reshape(1, width)  1.28 us

profile of v1, /device:TPU:0, one launch (start us, length us, event | category | flops | bytes accessed | tf_op | source)
XLA Modules:
  0.0 32.8 jit_solution(16424637546655582791)
XLA Ops:
  0.6 1.3 %reshape.13.refs_1_ = bf16[1,1024]{1,0:T(2,128)(2,1)} reshape(bf16[1024]{0:T(1024)(128)(2,1)} %param.10) | data formatting | bytes 4096 | tf_op jit(solution)/shard_map/reshape | solution.py:373
  1.9 28.1 %shard_map.104 = (bf16[8,32,1024]{2,1,0:T(8,128)(2,1)}, f32[4,4,64,128]{3,2,1,0:T(8,128)}) custom-call(bf16[8,32,1024]{2,1,0:T(8,128)(2,1)} %refs_0_.1, bf16[1,1024]{1,0:T(2,128)(2,1)} %reshape.13.refs_1_, bf16[1024,128]{1,0:T(8,128)(2,1)} %refs_2_.1, bf16[1024,128]{1,0:T(8,128)(2,1)} %refs_3_.1, bf16[1024,256]{1,0:T(8,128)(2,1)} %refs_4_.1, ...), custom_call_target="tpu_custom_call" | custom-call | tf_op jit(solution)/shard_map/pallas_call | solution.py:332
  30.1 0.0 copy-start
  30.1 1.9 %copy.13 = bf16[8,32,1024]{2,1,0:T(8,128)(2,1)} copy(bf16[8,32,1024]{2,1,0:T(8,128)(2,1)} %get-tuple-element.8) | data formatting | bytes 1048576
  32.0 0.0 copy-done
  32.0 0.8 %copy.14 = f32[8,2,64,128]{3,2,1,0:T(8,128)} copy(f32[8,2,64,128]{3,2,1,0:T(8,128)S(1)} %bitcast.2) | data formatting | bytes 1048576
Async XLA Ops:
  30.1 1.9 %copy-start = (f32[4,4,64,128]{3,2,1,0:T(8,128)S(1)}, f32[4,4,64,128]{3,2,1,0:T(8,128)}, u32[]{:S(2)}) copy-start(f32[4,4,64,128]{3,2,1,0:T(8,128)} %get-tuple-element.5) | copy-start | bytes 1572868

commit v2 on v1

--- a/solution.py
+++ b/solution.py
@@ -16,9 +16,9 @@
 
 def kernel(dims, *refs):
     (n_sp, n_tp, plane, column, heads) = dims
-    (x_hbm, gain_hbm, wq_hbm, wk_hbm, wv_hbm, wg_hbm, hgain_hbm, wo_hbm, init_hbm) = refs[:9]
+    (x_hbm, gain_ref, wq_hbm, wk_hbm, wv_hbm, wg_hbm, hgain_ref, wo_hbm, init_hbm) = refs[:9]
     out_ref, closing_ref = refs[9:11]
-    (xbuf, gain, wbuf, hgain, wobuf, initb, nbuf, qm, km, kw, vs, gs, inner, lb, ra, sb, rb, sc, rc, sd, rd,
+    (xbuf, wbuf, hgain, wobuf, initb, nbuf, qm, km, kw, vs, gs, inner, lb, ra, sb, rb, sc, rc, sd, rd,
      mx, mr, lsem, xs, xr, ws, wr, as_, ar, bs, br, cs, cr, ds_, dr, ms, mrs) = refs[11:]
     seqs, half, width = x_hbm.shape
     stretch = half * n_tp
@@ -60,12 +60,11 @@
 
     loads = [
         (x_hbm, xbuf.at[t_me]),
-        (gain_hbm, gain),
         (wq_hbm, wbuf.at[:, 0:kc]),
         (wk_hbm, wbuf.at[:, kc : 2 * kc]),
         (wv_hbm, wbuf.at[:, 2 * kc : 2 * kc + vc]),
         (wg_hbm, wbuf.at[:, 2 * kc + vc :]),
-        (hgain_hbm, hgain),
+        (hgain_ref, hgain),
         (init_hbm.at[p_me], initb),
         (wo_hbm, wobuf.at[t_me]),
     ]
@@ -73,6 +72,7 @@
     for c in local:
         c.start()
 
+    gain = gain_ref[...].reshape(1, width).astype(F32)
     def fiota(shape, dim):
         return lax.broadcasted_iota(jnp.int32, shape, dim).astype(F32)
 
@@ -103,27 +103,29 @@
         jnp.exp(jnp.maximum(gap, 0.0) * lg_of(rhead)),
         0.0,
     )
-    inner_decay = mask
-
-    pl.semaphore_wait(barrier, len(peers))
+
+
+    local[0].wait()
+    with jax.named_scope('w_barrier'):
+        pl.semaphore_wait(barrier, len(peers))
 
     sends = []
     for o in range(1, n_tp):
         j, where = in_chip(o)
-        sends.append(remote(x_hbm, xbuf.at[t_me], xs.at[j], xr.at[t_me], where))
-        sends.append(remote(wo_hbm, wobuf.at[t_me], ws.at[j], wr.at[t_me], where))
+        sends.append(remote(xbuf.at[t_me], xbuf.at[t_me], xs.at[j], xr.at[t_me], where))
     for c in sends:
         c.start()
 
-    for c in local[:6]:
-        c.wait()
+    with jax.named_scope('w_load'):
+        for c in local[1:5]:
+            c.wait()
 
     def project(t):
         for s in range(seqs):
             xf = xbuf[t, s].astype(F32)
             ms_ = jnp.mean(xf * xf, axis=-1, keepdims=True)
             nbuf[s * half : (s + 1) * half, :] = (
-                xf * lax.rsqrt(ms_ + EPS) * gain[...].astype(F32)
+                xf * lax.rsqrt(ms_ + EPS) * gain
             ).astype(BF16)
         pos0 = (t * half).astype(F32)
         angle = (me * stretch).astype(F32) + pos0 + sub
@@ -157,11 +159,14 @@
             vs[:, at, :] = v[:, h * dv : (h + 1) * dv].reshape(seqs, half, dv)
             gs[:, at, :] = g[:, h * dv : (h + 1) * dv].reshape(seqs, half, dv)
 
-    project(t_me)
+    with jax.named_scope('project_own'):
+        project(t_me)
     for o in range(1, n_tp):
         j, where = in_chip(o)
-        remote(x_hbm, xbuf.at[j], xs.at[j], xr.at[j], where).wait_recv()
-        project(j)
+        with jax.named_scope('w_x'):
+            remote(xbuf.at[j], xbuf.at[j], xs.at[j], xr.at[j], where).wait_recv()
+        with jax.named_scope('project_other'):
+            project(j)
 
     for s in range(seqs):
         state = lax.dot_general(
@@ -171,9 +176,24 @@
             c = s * heads + h
             lb[c // group, c % group] = state[h * dk : (h + 1) * dk]
 
-    for o in range(1, plane):
-        j, where = in_plane(o)
-        c = remote(lb.at[j], ra.at[p_me], as_.at[j], ar.at[p_me], where)
+    def to_plane(src, dst, ss, rs, g):
+        for o in range(1, plane):
+            j, where = in_plane(o)
+            c = remote(src(j), dst.at[p_me, g], ss.at[j, g], rs.at[p_me, g], where)
+            c.start()
+            sends.append(c)
+
+    def from_plane(dst, ss, rs, g):
+        for o in range(1, plane):
+            j, where = in_plane(o)
+            remote(dst.at[j, g], dst.at[j, g], ss.at[j, g], rs.at[j, g], where).wait_recv()
+
+    for g in range(group):
+        to_plane(lambda j: lb.at[j, g], ra, as_, ar, g)
+
+    for o in range(1, n_tp):
+        j, where = in_chip(o)
+        c = remote(wo_hbm, wobuf.at[t_me], ws.at[j], wr.at[t_me], where)
         c.start()
         sends.append(c)
 
@@ -181,11 +201,11 @@
         scores = lax.dot_general(
             qm[s], km[s], (((1,), (1,)), ((), ())), preferred_element_type=F32
         )
-        scores = (scores * inner_decay).astype(BF16)
+        scores = (scores * mask).astype(BF16)
         inner[s] = jnp.dot(scores, vs[s], preferred_element_type=F32)
 
     ra[p_me] = lb[p_me]
-    for c in local[6:]:
+    for c in local[5:]:
         c.wait()
 
     group_lg = []
@@ -197,21 +217,6 @@
         return jnp.exp(jnp.broadcast_to(group_lg[g] * k, (1, dv)))
 
     one_block = [power(g, 1.0) for g in range(group)]
-
-    for o in range(1, plane):
-        j, where = in_plane(o)
-        remote(lb.at[j], ra.at[j], as_.at[j], ar.at[j], where).wait_recv()
-    for g in range(group):
-        acc = ra[0, g].astype(F32)
-        for p in range(1, plane):
-            acc = acc * one_block[g] + ra[p, g].astype(F32)
-        sb[g] = acc.astype(BF16)
-    for o in range(1, column):
-        j, where = in_column(o)
-        c = remote(sb, rb.at[z_me], bs.at[j], br.at[z_me], where)
-        c.start()
-        sends.append(c)
-    rb[z_me] = sb[...]
 
     zf = z_me.astype(F32)
     before = [
@@ -225,10 +230,25 @@
     after = [[power(g, float(plane * (column - 1 - z))) for z in range(column)] for g in range(group)]
     whole = [power(g, float(plane * column)) for g in range(group)]
 
-    for o in range(1, column):
-        j, where = in_column(o)
-        remote(sb, rb.at[j], bs.at[j], br.at[j], where).wait_recv()
-    for g in range(group):
+    for g in range(group):
+        with jax.named_scope('w_a'):
+            from_plane(ra, as_, ar, g)
+        acc = ra[0, g].astype(F32)
+        for p in range(1, plane):
+            acc = acc * one_block[g] + ra[p, g].astype(F32)
+        sb[g] = acc.astype(BF16)
+        for o in range(1, column):
+            j, where = in_column(o)
+            c = remote(sb.at[g], rb.at[z_me, g], bs.at[j, g], br.at[z_me, g], where)
+            c.start()
+            sends.append(c)
+        rb[z_me, g] = sb[g]
+
+    for g in range(group):
+        with jax.named_scope('w_b'):
+            for o in range(1, column):
+                j, where = in_column(o)
+                remote(sb.at[g], rb.at[j, g], bs.at[j, g], br.at[j, g], where).wait_recv()
         start = initb[g]
         incoming = start * first[g]
         total = start * whole[g]
@@ -241,18 +261,10 @@
             if p < plane - 1:
                 incoming = incoming * one_block[g] + ra[p, g].astype(F32)
         sd[g] = total.astype(BF16)
-    for o in range(1, plane):
-        j, where = in_plane(o)
-        c = remote(sc.at[j], rc.at[p_me], cs.at[j], cr.at[p_me], where)
-        c.start()
-        sends.append(c)
-    for o in range(1, plane):
-        j, where = in_plane(o)
-        c = remote(sd, rd.at[p_me], ds_.at[j], dr.at[p_me], where)
-        c.start()
-        sends.append(c)
-    rc[p_me] = sc[p_me]
-    rd[p_me] = sd[...]
+        to_plane(lambda j: sc.at[j, g], rc, cs, cr, g)
+        to_plane(lambda j: sd.at[g], rd, ds_, dr, g)
+        rc[p_me, g] = sc[p_me, g]
+        rd[p_me, g] = sd[g]
 
     gain_rows = jnp.concatenate(
         [
@@ -262,45 +274,50 @@
         axis=0,
     )
 
-    for o in range(1, plane):
-        j, where = in_plane(o)
-        remote(sc.at[j], rc.at[j], cs.at[j], cr.at[j], where).wait_recv()
-
-    def finish(t):
+    half_pos, half_head = places_of(fiota((rows_half, dv), 0))
+
+    def finish(t, s):
         at = pl.ds(pl.multiple_of(t * rows_half, rows_half), rows_half)
-        hpos, hhead = places_of(fiota((rows_half, dv), 0))
-        decay = jnp.exp((hpos + (t * half).astype(F32) + 1.0) * lg_of(hhead))
-        for s in range(seqs):
-            memory = jnp.concatenate(
-                [rc[(s * heads + h) // group, (s * heads + h) % group] for h in range(heads)], axis=0
-            )
-            cross = jnp.dot(qm[s, at, :], memory, preferred_element_type=F32)
-            kept = inner[s, at, :] + cross * decay
-            centre = jnp.mean(kept, axis=-1, keepdims=True)
-            kept = kept - centre
-            spread = jnp.mean(kept * kept, axis=-1, keepdims=True)
-            gate = gs[s, at, :].astype(F32)
-            gate = gate * jax.nn.sigmoid(gate)
-            mx[t, s] = (gate * (kept * lax.rsqrt(spread + EPS) * gain_rows)).astype(BF16)
-
-    for o in range(1, n_tp):
-        j, where = in_chip(o)
-        finish(j)
-        c = remote(mx.at[j], mr.at[t_me], ms.at[j], mrs.at[t_me], where)
-        c.start()
-        sends.append(c)
-    finish(t_me)
+        decay = jnp.exp((half_pos + (t * half).astype(F32) + 1.0) * lg_of(half_head))
+        memory = jnp.concatenate(
+            [rc[(s * heads + h) // group, (s * heads + h) % group] for h in range(heads)], axis=0
+        )
+        cross = jnp.dot(qm[s, at, :], memory, preferred_element_type=F32)
+        kept = inner[s, at, :] + cross * decay
+        centre = jnp.mean(kept, axis=-1, keepdims=True)
+        kept = kept - centre
+        spread = jnp.mean(kept * kept, axis=-1, keepdims=True)
+        gate = gs[s, at, :].astype(F32)
+        gate = gate * jax.nn.sigmoid(gate)
+        mx[t, s] = (gate * (kept * lax.rsqrt(spread + EPS) * gain_rows)).astype(BF16)
+
+    needs = [max((s * heads + h) % group for h in range(heads)) for s in range(seqs)]
+    for g in range(group):
+        with jax.named_scope('w_c'):
+            from_plane(rc, cs, cr, g)
+        ready = [s for s in range(seqs) if needs[s] == g]
+        for o in range(1, n_tp):
+            j, where = in_chip(o)
+            for s in ready:
+                finish(j, s)
+            if g == group - 1:
+                c = remote(mx.at[j], mr.at[t_me], ms.at[j], mrs.at[t_me], where)
+                c.start()
+                sends.append(c)
+        for s in ready:
+            finish(t_me, s)
     mr[t_me] = mx[t_me]
 
-    for o in range(1, plane):
-        j, where = in_plane(o)
-        remote(sd, rd.at[j], ds_.at[j], dr.at[j], where).wait_recv()
+    for g in range(group):
+        with jax.named_scope('w_d'):
+            from_plane(rd, ds_, dr, g)
     closing_ref[...] = rd[...].astype(F32)
 
     for o in range(1, n_tp):
         j, where = in_chip(o)
         remote(wo_hbm, wobuf.at[j], ws.at[j], wr.at[j], where).wait_recv()
-        remote(mx.at[j], mr.at[j], ms.at[j], mrs.at[j], where).wait_recv()
+        with jax.named_scope('w_m'):
+            remote(mx.at[j], mr.at[j], ms.at[j], mrs.at[j], where).wait_recv()
     side = jnp.concatenate(
         [
             mr[t, :, h * half : (h + 1) * half, :].reshape(seqs * half, dv)
@@ -335,11 +352,10 @@
             jax.ShapeDtypeStruct((seqs, half, width), BF16),
             jax.ShapeDtypeStruct((plane,) + state, F32),
         ),
-        in_specs=[any_spec] * 9,
+        in_specs=[any_spec, vmem_spec] + [any_spec] * 7,
         out_specs=(vmem_spec, vmem_spec),
         scratch_shapes=[
             V((n_tp, seqs, half, width), BF16),
-            V((1, width), BF16),
             V((width, 2 * kc + 2 * vc), BF16),
             V((heads, dv), BF16),
             V((n_tp, vc, width), BF16),
@@ -361,16 +377,16 @@
             V((plane,) + state, BF16),
             V((n_tp, seqs, heads * half, dv), BF16),
             V((n_tp, seqs, heads * half, dv), BF16),
-            D((9,)),
+            D((8,)),
             D((n_tp,)), D((n_tp,)), D((n_tp,)), D((n_tp,)),
-            D((plane,)), D((plane,)),
-            D((column,)), D((column,)),
-            D((plane,)), D((plane,)),
-            D((plane,)), D((plane,)),
+            D((plane, group)), D((plane, group)),
+            D((column, group)), D((column, group)),
+            D((plane, group)), D((plane, group)),
+            D((plane, group)), D((plane, group)),
             D((n_tp,)), D((n_tp,)),
         ],
         compiler_params=pltpu.CompilerParams(collective_id=0, has_side_effects=True),
-    )(x, gain.reshape(1, width), wq, wk, wv, wg, hgain, wo, init.reshape((plane,) + state))
+    )(x, gain, wq, wk, wv, wg, hgain, wo, init.reshape((plane,) + state))
     return out, closing.reshape(init.shape)
 
 

time: 33 us -> 30.3 us (0.918)
  Pallas kernels: 28.1 us -> 26.5 us
  local copies, waits for them, and re-layouts: 4 us -> 2.72 us
    pallas_call x1, Pallas kernels: 28.1 us -> 26.5 us  [on_device(): pl.pallas_call(functools.partial(kernel, (n_sp, n_tp, plane, column, head...]
    reshape x1 -> x0, local copies, waits for them, and re-layouts: 1.28 us -> none  [on_device(): gain.reshape(1, width)]
where the time goes in v2:
time: 30.3 us; the launch traced here: 29.9 us
  Pallas kernels  26.5 us (87%)
  local copies, waits for them, and re-layouts  2.72 us (9%)
  between operations  0.65 us (2%)
    pallas_call x1, Pallas kernels, on_device(): pl.pallas_call(functools.partial(kernel, (n_sp, n_tp, plane, column, head...  26.5 us
    unnamed x4, local copies, waits for them, and re-layouts  2.72 us

profile of v2, /device:TPU:0, one launch (start us, length us, event | category | flops | bytes accessed | tf_op | source)
XLA Modules:
  0.0 29.9 jit_solution(10794415942155263906)
XLA Ops:
  0.6 26.5 %shard_map.104 = (bf16[8,32,1024]{2,1,0:T(8,128)(2,1)}, f32[4,4,64,128]{3,2,1,0:T(8,128)}) custom-call(bf16[8,32,1024]{2,1,0:T(8,128)(2,1)} %refs_0_.1, bf16[1024]{0:T(1024)(128)(2,1)} %refs_1_.1, bf16[1024,128]{1,0:T(8,128)(2,1)} %refs_2_.1, bf16[1024,128]{1,0:T(8,128)(2,1)} %refs_3_.1, bf16[1024,256]{1,0:T(8,128)(2,1)} %refs_4_.1, ...), custom_call_target="tpu_custom_call" | custom-call | tf_op jit(solution)/shard_map/pallas_call | solution.py:349
  27.1 0.0 copy-start
  27.2 1.9 %copy.13 = bf16[8,32,1024]{2,1,0:T(8,128)(2,1)} copy(bf16[8,32,1024]{2,1,0:T(8,128)(2,1)} %get-tuple-element.8) | data formatting | bytes 1048576
  29.1 0.0 copy-done
  29.1 0.8 %copy.14 = f32[8,2,64,128]{3,2,1,0:T(8,128)} copy(f32[8,2,64,128]{3,2,1,0:T(8,128)S(1)} %bitcast.2) | data formatting | bytes 1048576
Async XLA Ops:
  27.1 1.9 %copy-start = (f32[4,4,64,128]{3,2,1,0:T(8,128)S(1)}, f32[4,4,64,128]{3,2,1,0:T(8,128)}, u32[]{:S(2)}) copy-start(f32[4,4,64,128]{3,2,1,0:T(8,128)} %get-tuple-element.5) | copy-start | bytes 1572868
